TPU v7x, 512 devices: a whole 4x8x8 slice. The times are simulated.
512 devices in a mesh: sp: 64 (over z, y), fs: 4 (over x), tp: 2 (over core).
Axes of the slice: x: 4, y: 8, z: 8, core: 2. Of those that a mesh axis runs over, the one named last changes fastest.
Arguments:
- tokens: bfloat16 [4, 8192, 2048], P('fs', ('sp', 'tp')), may hold values from -6 to 6
- norm_gain: float32 [2048], replicated, may hold values from 0.1 to 1.9
- gla_query_weight: bfloat16 [2048, 512], P('sp', 'tp'), may hold values from -0.125 to 0.125
- gla_key_weight: bfloat16 [2048, 512], P('sp', 'tp'), may hold values from -0.125 to 0.125
- gla_value_weight: bfloat16 [2048, 1024], P('sp', 'tp'), may hold values from -0.125 to 0.125
- decay_down: bfloat16 [2048, 32], P('sp'), may hold values from -0.125 to 0.125
- decay_up: bfloat16 [32, 512], P(None, 'tp'), may hold values from -1 to 1
- decay_bias: float32 [512], P('tp'), may hold values from 0.5 to 12
- head_gain: float32 [128], replicated, may hold values from 0.1 to 1.9
- window_query_weight: bfloat16 [2048, 1024], P('sp', 'tp'), may hold values from -3 to 3
- window_key_weight: bfloat16 [2048, 256], P('sp', 'tp'), may hold values from -3 to 3
- window_value_weight: bfloat16 [2048, 256], P('sp', 'tp'), may hold values from -0.125 to 0.125
- sink_logit: float32 [16], P('tp'), may hold values from 3 to 7
- gla_output_weight: bfloat16 [1024, 2048], P('tp', 'sp'), may hold values from -0.125 to 0.125
- window_output_weight: bfloat16 [1024, 2048], P('tp', 'sp'), may hold values from -0.125 to 0.125
Outputs:
- mixed: bfloat16 [4, 8192, 2048], P('fs', ('sp', 'tp'))
All inputs are finite; a program needn't handle non-finite values.
Results may differ from a plain program's by a relative error of at most 0.013.
Values may be sent and summed in bfloat16 or wider, within the bound.
A program may use at most 64 MiB of HBM per device.

v0:
```python
import jax
import jax.numpy as jnp
from jax import lax
from jax.sharding import Mesh
from jax.sharding import PartitionSpec as P

KEY_DIM = 64
VALUE_DIM = 128
HEAD_DIM = 64
WINDOW = 128
SPAN = 64
SP = ("sp_0", "sp_1")
SP_TP = ("sp_0", "sp_1", "tp")
GROUP = ("fs", "tp")
EPS = 1e-06
SOFTMAX_TEMPER = 16.0
HIGH = lax.Precision.HIGHEST


def rms_rows(values, gain):
    mean_square = jnp.mean(values * values, axis=-1, keepdims=True)
    return values * lax.rsqrt(mean_square + EPS) * gain


def own_part(value, at, size, dim):
    return lax.dynamic_slice_in_dim(value, at * size, size, axis=dim)


def combine(earlier, later):
    return (later[1][..., None] * earlier[0] + later[0], earlier[1] * later[1])


def carried_in(value):
    start = (jnp.zeros_like(value[0]), jnp.ones_like(value[1]))
    before, subtotal = (start, value)
    for axis in ("sp_1", "sp_0"):
        peers, place = (lax.axis_size(axis), lax.axis_index(axis))
        both = jnp.concatenate(
            [subtotal[0], jnp.broadcast_to(subtotal[1][..., None], subtotal[0].shape[:-1] + (1,))],
            -1,
        )
        pieces = lax.all_gather(both, axis)
        inside, subtotal = (start, start)
        for k in range(peers):
            subtotal = combine(subtotal, (pieces[k, ..., :-1], pieces[k, ..., -1]))
            inside = jax.tree.map(lambda n, o: jnp.where(k < place, n, o), subtotal, inside)
        before = combine(inside, before)
    return before[0]


def per_device(
    tokens,
    norm_gain,
    gla_query_weight,
    gla_key_weight,
    gla_value_weight,
    decay_down,
    decay_up,
    decay_bias,
    head_gain,
    window_query_weight,
    window_key_weight,
    window_value_weight,
    sink_logit,
    gla_output_weight,
    window_output_weight,
):
    x = lax.axis_index("fs")
    rows = lax.all_gather(tokens[0], GROUP, axis=0, tiled=True)
    w_in = jnp.concatenate(
        [
            own_part(gla_query_weight, x, 64, 1),
            own_part(gla_key_weight, x, 64, 1),
            own_part(gla_value_weight, x, 128, 1),
            own_part(window_query_weight, x, 128, 1),
            own_part(window_key_weight, x // 2, 64, 1),
            own_part(window_value_weight, x // 2, 64, 1),
            decay_down,
        ],
        axis=1,
    )
    w_in = lax.all_gather(w_in, SP, axis=0, tiled=True)
    w_out = jnp.concatenate(
        [own_part(gla_output_weight, x, 128, 0), own_part(window_output_weight, x, 128, 0)], axis=0
    ).T
    w_out = lax.all_gather(w_out, SP, axis=0, tiled=True)
    normed = rms_rows(rows.astype(jnp.float32), norm_gain).astype(jnp.bfloat16)
    proj = jnp.dot(normed, w_in, preferred_element_type=jnp.float32).astype(jnp.bfloat16)
    seqs = 4
    spans = rows.shape[0] // seqs // SPAN
    gate = jnp.dot(proj[:, 512:], own_part(decay_up, x, 64, 1), preferred_element_type=jnp.float32)
    log_rate = jax.nn.log_sigmoid(gate + own_part(decay_bias, x, 64, 0)) / SOFTMAX_TEMPER

    def blocks(v):
        return v.astype(jnp.float32).reshape(seqs, spans, SPAN, -1)

    q, k, v = (
        blocks(proj[:, :64]) * KEY_DIM ** (-0.5),
        blocks(proj[:, 64:128]),
        blocks(proj[:, 128:256]),
    )
    within = jnp.cumsum(blocks(log_rate), axis=2)
    block_total = within[:, :, -1]
    q_dec = q * jnp.exp(within)
    k_dec = k * jnp.exp(-within)
    k_end = k * jnp.exp(block_total[:, :, None] - within)
    scores = jnp.einsum("snid,snjd->snij", q_dec, k_dec, precision=HIGH)
    scores = jnp.where(jnp.tril(jnp.ones((SPAN, SPAN), bool)), scores, 0.0)
    local_out = jnp.einsum("snij,snje->snie", scores, v, precision=HIGH)
    update = jnp.einsum("snjd,snje->snde", k_end, v, precision=HIGH)
    decay = jnp.exp(block_total)
    last_state = decay[:, 1, :, None] * update[:, 0] + update[:, 1]
    incoming = carried_in((last_state, decay[:, 0] * decay[:, 1]))
    entering = jnp.stack([incoming, decay[:, 0, :, None] * incoming + update[:, 0]], axis=1)
    wq = proj[:, 256:384].reshape(seqs, WINDOW, 2, HEAD_DIM)
    wkv = proj[:, 384:512].reshape(seqs, WINDOW, 2 * HEAD_DIM)
    ny, nz = (lax.axis_size("sp_1"), lax.axis_size("sp_0"))
    n = ny * nz
    edge = lax.ppermute(wkv, SP, [(i, i + 1) for i in range(n - 1)])
    band = jnp.concatenate([edge, wkv], axis=1)
    s = jnp.einsum("sqhd,skd->shqk", wq, band[..., :64], preferred_element_type=jnp.float32)
    s = s * HEAD_DIM ** (-0.5)
    dist = jnp.arange(WINDOW)[:, None] + WINDOW - jnp.arange(2 * WINDOW)[None]
    ok = (dist >= 0) & (dist < WINDOW)
    ok = ok & ((lax.axis_index(SP) > 0) | (jnp.arange(2 * WINDOW)[None] >= WINDOW))
    s = jnp.where(ok, s, -1e30)
    sink = own_part(sink_logit, x, 2, 0)[None, :, None, None]
    top = jnp.maximum(jnp.max(s, -1, keepdims=True), sink)
    e = jnp.exp(s - top)
    den = jnp.sum(e, -1, keepdims=True) + jnp.exp(sink - top)
    att = jnp.einsum(
        "shqk,skd->sqhd",
        (e / den).astype(jnp.bfloat16),
        band[..., 64:],
        preferred_element_type=jnp.float32,
    ).astype(jnp.bfloat16)
    gla_out = local_out + jnp.einsum("snid,snde->snie", q_dec, entering, precision=HIGH)
    hidden = rms_rows(gla_out, head_gain).astype(jnp.bfloat16).reshape(-1, VALUE_DIM)
    hidden = jnp.concatenate([hidden, att.reshape(-1, 128)], axis=1)
    total = jnp.einsum("rk,nk->rn", hidden, w_out, preferred_element_type=jnp.float32)
    total = total.astype(jnp.bfloat16).reshape(8, -1, total.shape[1])
    arrived = lax.all_to_all(total, GROUP, split_axis=0, concat_axis=0, tiled=True)
    return arrived.astype(jnp.float32).sum(axis=0).astype(jnp.bfloat16)[None]


def solution(mesh):
    split = Mesh(
        mesh.devices.reshape(8, 8, mesh.shape["fs"], mesh.shape["tp"]), ("sp_0", "sp_1", "fs", "tp")
    )
    return jax.shard_map(
        per_device,
        mesh=split,
        in_specs=(
            P("fs", SP_TP, None),
            P(),
            P(SP, "tp"),
            P(SP, "tp"),
            P(SP, "tp"),
            P(SP, None),
            P(None, "tp"),
            P("tp"),
            P(),
            P(SP, "tp"),
            P(SP, "tp"),
            P(SP, "tp"),
            P("tp"),
            P("tp", SP),
            P("tp", SP),
        ),
        out_specs=P("fs", SP_TP, None),
        check_vma=False,
    )
```

profile of v0, /device:TPU:1, one launch (start us, length us, event | category | flops | bytes accessed | tf_op | source)
XLA Modules:
  0.0 351.1 jit_solution(2613073268380290763)
XLA Ops:
  6.5 0.7 all-gather.13.cloned.1.call-update
  7.3 0.8 constant_dynamic-slice_fusion.2
  8.1 0.8 constant_dynamic-slice_fusion.6
  8.9 0.7 constant_dynamic-slice_fusion.4
  9.6 1.4 concatenate.18
  11.1 0.8 dynamic_slice.40
  11.9 34.1 %all-gather.13.cloned.1.call-done = bf16[1,512,2048]{2,1,0:T(8,128)(2,1)} async-done(((bf16[1,64,2048]{2,1,0:T(8,128)(2,1)}), bf16[1,512,2048]{2,1,0:T(8,128)(2,1)}) %all-gather.13.cloned.1.call-update) | async-done | bytes 2097168 | tf_op jit(solution)/shard_map/all_gather | solution.py:69
  46.0 2.2 fusion
  48.2 81.3 %all-gather.9.cloned.1.call-done = bf16[2048,544]{1,0:T(8,128)(2,1)} async-done(((bf16[32,544]{1,0:T(8,128)(2,1)}), bf16[2048,544]{1,0:T(8,128)(2,1)}) %all-gather.9.cloned.1.call-update) | async-done | bytes 2228240 | tf_op jit(solution)/shard_map/all_gather | solution.py:82
  129.5 3.2 fusion.10
  132.8 0.8 copy-done.3
  134.7 0.4 fusion.20
  135.3 0.7 pad_maximum_fusion
  136.1 40.0 %all-gather.15.cloned.1.call-done = f32[32,64,129]{2,1,0:T(8,128)} async-done(((f32[4,64,129]{2,1,0:T(8,128)}), f32[32,64,129]{2,1,0:T(8,128)}) %all-gather.15.cloned.1.call-update) | async-done | bytes 1056784 | tf_op jit(solution)/shard_map/all_gather | solution.py:42
  176.1 1.6 slice_reduce_fusion.7
  177.7 1.6 bitcast_add_fusion.9
  179.4 0.7 pad_maximum_fusion.1
  180.2 0.7 constant_dynamic-slice_fusion
  180.9 0.6 maximum_bitcast_fusion
  181.8 0.9 convert_multiply_fusion.2
  182.8 2.7 collective-permute-start
  185.5 0.6 convolution_select_fusion
  186.4 1.0 collective-permute-done
  187.5 0.4 fusion.63
  188.6 34.4 %all-gather.17.cloned.1.call-done = f32[32,64,129]{2,1,0:T(8,128)} async-done(((f32[4,64,129]{2,1,0:T(8,128)}), f32[32,64,129]{2,1,0:T(8,128)}) %all-gather.17.cloned.1.call-update) | async-done | bytes 1056784 | tf_op jit(solution)/shard_map/all_gather | solution.py:42
  223.1 1.6 slice_reduce_fusion.6
  224.7 2.0 bitcast_add_fusion
  226.7 0.5 multiply_reduce_fusion
  227.5 78.2 %all-gather.11.cloned.1.call-done = bf16[2048,256]{1,0:T(8,128)(2,1)} async-done(((bf16[32,256]{1,0:T(8,128)(2,1)}), bf16[2048,256]{1,0:T(8,128)(2,1)}) %all-gather.11.cloned.1.call-update) | async-done | bytes 1048592 | tf_op jit(solution)/shard_map/all_gather | solution.py:86
  305.7 2.0 convolution_convert_fusion
  307.7 35.7 %all_to_all.5 = bf16[8,64,2048]{2,1,0:T(8,128)(2,1)S(1)} all-to-all(bf16[8,64,2048]{2,1,0:T(8,128)(2,1)S(1)} %bitcast.222), channel_id=1, replica_groups=mesh['sp_0'=8,'sp_1'=8,'fs'=4,'tp'=2] {'fs','tp'}, dimensions={0} | all-to-all | bytes 4194304 | tf_op jit(solution)/shard_map/all_to_all | solution.py:142
  343.4 1.1 reduce_sum.42
  (56 shorter events, 3.2 us)
Async XLA Ops:
  6.5 127.0 %copy-start = (bf16[32,256]{1,0:T(8,128)(2,1)S(1)}, bf16[32,256]{1,0:T(8,128)(2,1)}, u32[]{:S(2)}) copy-start(bf16[32,256]{1,0:T(8,128)(2,1)} %param.21) | copy-start | bytes 49156
  6.5 123.0 %copy-start.5 = (f32[2048]{0:T(1024)S(1)}, f32[2048]{0:T(1024)}, u32[]{:S(2)}) copy-start(f32[2048]{0:T(1024)} %param.16) | copy-start | bytes 24580
  6.5 39.5 %all-gather.13.cloned.1.call-start = ((), (), s32[]{:S(2)}) async-start(), calls=%async_computation.3 | async-start | bytes 2359296 | tf_op jit(solution)/shard_map/all_gather | solution.py:69
  7.3 122.2 %all-gather.9.cloned.1.call-start = ((), (), s32[]{:S(2)}) async-start(), calls=%async_computation.1 | async-start | bytes 2662400 | tf_op jit(solution)/shard_map/all_gather | solution.py:82
  11.1 165.0 %all-gather.15.cloned.1.call-start = ((), (), s32[]{:S(2)}) async-start(), calls=%async_computation.4 | async-start | bytes 2359296 | tf_op jit(solution)/shard_map/all_gather | solution.py:42
  46.0 83.5 %copy-start.2 = (bf16[1,512,2048]{2,1,0:T(8,128)(2,1)S(1)}, bf16[1,512,2048]{2,1,0:T(8,128)(2,1)}, u32[]{:S(2)}) copy-start(bf16[1,512,2048]{2,1,0:T(8,128)(2,1)} %all-gather.13.cloned.1.call-done) | copy-start | bytes 6291460
  132.8 0.8 copy-start.3
  135.2 46.5 %copy-start.6 = (f32[8]{0:T(128)S(1)}, f32[8]{0:T(128)}, u32[]{:S(2)}) copy-start(f32[8]{0:T(128)} %param.27) | copy-start | bytes 100
  136.0 87.1 %all-gather.17.cloned.1.call-start = ((), (), s32[]{:S(2)}) async-start(), calls=%async_computation.5 | async-start | bytes 2359296 | tf_op jit(solution)/shard_map/all_gather | solution.py:42
  180.1 125.6 %all-gather.11.cloned.1.call-start = ((), (), s32[]{:S(2)}) async-start(), calls=%async_computation.2 | async-start | bytes 1064960 | tf_op jit(solution)/shard_map/all_gather | solution.py:86
  182.8 4.6 %collective-permute-start = (bf16[4,128,128]{1,2,0:T(8,128)(2,1)S(1)}, bf16[4,128,128]{1,2,0:T(8,128)(2,1)S(1)}, u32[]{:S(2)}, u32[]{:S(2)}) collective-permute-start(bf16[4,128,128]{1,2,0:T(8,128)(2,1)S(1)} %bitcast.238), channel_id=1, source_target_pairs={{0,8},{8,16},{16,24},{24,32},{32,40},{40,48},{48,56},{56,64},{64,7... | collective-permute-start | bytes 393224 | tf_op jit(solution)/shard_map/ppermute | solution.py:119
  188.2 36.6 %copy-start.1 = (f32[32,64,129]{2,1,0:T(8,128)S(1)}, f32[32,64,129]{2,1,0:T(8,128)}, u32[]{:S(2)}) copy-start(f32[32,64,129]{2,1,0:T(8,128)} %all-gather.15.cloned.1.call-done) | copy-start | bytes 3170308
  224.7 2.5 copy-start.4
Sparse Core Ops, SparseCore 0:
  9.5 36.4 all-gather.12
  49.0 80.4 all-gather.8
  136.1 39.8 all-gather.14
  180.2 42.7 all-gather.16
  226.0 79.6 all-gather.10
where the time goes:
time: 352 us; the launch traced here: 351 us
  waiting for transfers between devices  270 us (77%)
  blocking collectives  35.7 us (10%)
  other arithmetic  14.1 us (4%)
  between operations  13.5 us (4%)
  matrix products  8.02 us (2%)
  local copies, waits for them, and re-layouts  7.07 us (2%)
    all_gather x1, waiting for transfers between devices, per_device(): w_in = lax.all_gather(w_in, SP, axis=0, tiled=True)  81.3 us
    all_gather x1, waiting for transfers between devices, per_device(): w_out = lax.all_gather(w_out, SP, axis=0, tiled=True)  78.2 us
    all_gather x2, waiting for transfers between devices, carried_in(): pieces = lax.all_gather(both, axis)  74.4 us
    all_to_all x1, blocking collectives, per_device(): lax.all_to_all(total, GROUP, split_axis=0, concat_axis=0, tiled=True)  35.7 us
    all_gather x1, waiting for transfers between devices, per_device(): rows = lax.all_gather(tokens[0], GROUP, axis=0, tiled=True)  34.1 us
  transfers between devices with their start and end apart: 6, of which 6 were waited for; matrix products, arithmetic and copies ran while one was open for 4% of the time, Pallas kernels for 0%

commit v1 on v0

--- a/solution.py
+++ b/solution.py
@@ -79,11 +79,14 @@
         ],
         axis=1,
     )
-    w_in = lax.all_gather(w_in, SP, axis=0, tiled=True)
     w_out = jnp.concatenate(
         [own_part(gla_output_weight, x, 128, 0), own_part(window_output_weight, x, 128, 0)], axis=0
     ).T
-    w_out = lax.all_gather(w_out, SP, axis=0, tiled=True)
+    w_in, w_out = jnp.split(
+        lax.all_gather(jnp.concatenate([w_in, w_out], axis=1), SP, axis=0, tiled=True),
+        [w_in.shape[1]],
+        axis=1,
+    )
     normed = rms_rows(rows.astype(jnp.float32), norm_gain).astype(jnp.bfloat16)
     proj = jnp.dot(normed, w_in, preferred_element_type=jnp.float32).astype(jnp.bfloat16)
     seqs = 4

time: 352 us -> 274 us (0.78)
  waiting for transfers between devices: 270 us -> 195 us
    all_gather x2 -> x1, waiting for transfers between devices: 159 us -> 82.7 us  [per_device(): lax.all_gather(jnp.concatenate([w_in, w_out], axis=1), SP, axis=0, tiled=...]
  transfers between devices with their start and end apart: 6 -> 5, of which waited for: 6 -> 4; matrix products, arithmetic and copies ran while one was open for 4% -> 5% of each run, Pallas kernels for 0% -> 0%
where the time goes in v1:
time: 274 us
  waiting for transfers between devices  195 us (71%)
  blocking collectives  35 us (13%)
  between operations  13.5 us (5%)
  other arithmetic  12.6 us (5%)
  matrix products  8.62 us (3%)
  local copies, waits for them, and re-layouts  6.31 us (2%)
  starting transfers between devices  2.85 us (1%)
    all_gather x1, waiting for transfers between devices, per_device(): lax.all_gather(jnp.concatenate([w_in, w_out], axis=1), SP, axis=0, tiled=...  82.7 us
    all_gather x2, waiting for transfers between devices, carried_in(): pieces = lax.all_gather(both, axis)  77.8 us
    all_to_all x1, blocking collectives, per_device(): lax.all_to_all(total, GROUP, split_axis=0, concat_axis=0, tiled=True)  35 us
    all_gather x1, waiting for transfers between devices, per_device(): rows = lax.all_gather(tokens[0], GROUP, axis=0, tiled=True)  33.4 us
  transfers between devices with their start and end apart: 5, of which 4 were waited for; matrix products, arithmetic and copies ran while one was open for 5% of the time, Pallas kernels for 0%

profile of v1, /device:TPU:1, one launch (start us, length us, event | category | flops | bytes accessed | tf_op | source)
XLA Modules:
  0.0 273.6 jit_solution(7847653949215843220)
XLA Ops:
  6.5 0.7 all-gather.10.cloned.1.call-update
  7.3 0.7 constant_dynamic-slice_fusion.4
  8.1 0.7 constant_dynamic-slice_fusion
  8.8 0.8 constant_dynamic-slice_fusion.6
  9.6 0.8 constant_dynamic-slice_fusion.2
  10.4 1.4 concatenate.19
  11.8 0.8 dynamic_slice.42
  12.6 33.4 %all-gather.10.cloned.1.call-done = bf16[1,512,2048]{2,1,0:T(8,128)(2,1)} async-done(((bf16[1,64,2048]{2,1,0:T(8,128)(2,1)}), bf16[1,512,2048]{2,1,0:T(8,128)(2,1)}) %all-gather.10.cloned.1.call-update) | async-done | bytes 2097168 | tf_op jit(solution)/shard_map/all_gather | solution.py:69
  46.0 2.2 fusion
  48.2 82.7 %all-gather.8.cloned.1.call-done = bf16[2048,800]{1,0:T(8,128)(2,1)} async-done(((bf16[32,800]{1,0:T(8,128)(2,1)}), bf16[2048,800]{1,0:T(8,128)(2,1)}) %all-gather.8.cloned.1.call-update) | async-done | bytes 3276816 | tf_op jit(solution)/shard_map/all_gather | solution.py:86
  131.0 3.2 %fusion.11 = bf16[512,544]{0,1:T(8,128)(2,1)S(1)} fusion(bf16[2048,800]{1,0:T(8,128)(2,1)} %all-gather.8.cloned.1.call-done, bf16[1,512,2048]{2,1,0:T(8,128)(2,1)S(1)} %copy-done.2, f32[2048]{0:T(1024)S(1)} %copy-done.4, f32[512]{0:T(512)S(1)} %add_rsqrt_fusion.1), kind=kOutput, calls=%fused_computation.14 | convolution fusion | flops 1145323520 | bytes 5285888 | tf_op jit(solution)/shard_map/dot_general | solution.py:91
  134.4 0.4 fusion.32
  135.1 0.2 reduce_window_sum.11
  135.5 0.4 fusion.24
  136.0 0.7 pad_maximum_fusion
  137.1 2.7 collective-permute-start
  140.0 36.9 %all-gather.12.cloned.1.call-done = f32[32,64,129]{2,1,0:T(8,128)} async-done(((f32[4,64,129]{2,1,0:T(8,128)}), f32[32,64,129]{2,1,0:T(8,128)}) %all-gather.12.cloned.1.call-update) | async-done | bytes 1056784 | tf_op jit(solution)/shard_map/all_gather | solution.py:42
  176.9 1.6 slice_reduce_fusion.7
  178.6 1.6 bitcast_add_fusion.9
  180.2 0.7 pad_maximum_fusion.1
  181.0 0.6 convolution_select_fusion
  181.6 0.3 fusion.68
  181.9 0.4 fusion.67
  182.3 0.2 fusion.19
  182.6 0.3 fusion.16
  183.1 40.9 %all-gather.14.cloned.1.call-done = f32[32,64,129]{2,1,0:T(8,128)} async-done(((f32[4,64,129]{2,1,0:T(8,128)}), f32[32,64,129]{2,1,0:T(8,128)}) %all-gather.14.cloned.1.call-update) | async-done | bytes 1056784 | tf_op jit(solution)/shard_map/all_gather | solution.py:42
  223.9 1.6 slice_reduce_fusion.6
  225.6 2.0 bitcast_add_fusion
  227.5 0.5 multiply_reduce_fusion
  228.4 2.6 convolution_convert_fusion
  230.9 35.0 %all_to_all.5 = bf16[8,64,2048]{2,1,0:T(8,128)(2,1)S(1)} all-to-all(bf16[8,64,2048]{2,1,0:T(8,128)(2,1)S(1)} %bitcast.220), channel_id=1, replica_groups=mesh['sp_0'=8,'sp_1'=8,'fs'=4,'tp'=2] {'fs','tp'}, dimensions={0} | all-to-all | bytes 4194304 | tf_op jit(solution)/shard_map/all_to_all | solution.py:145
  266.0 1.1 reduce_sum.42
  (51 shorter events, 1.9 us)
Async XLA Ops:
  6.5 127.9 %copy-start = (bf16[32,256]{1,0:T(8,128)(2,1)S(1)}, bf16[32,256]{1,0:T(8,128)(2,1)}, u32[]{:S(2)}) copy-start(bf16[32,256]{1,0:T(8,128)(2,1)} %param.21) | copy-start | bytes 49156
  6.5 124.4 %copy-start.4 = (f32[2048]{0:T(1024)S(1)}, f32[2048]{0:T(1024)}, u32[]{:S(2)}) copy-start(f32[2048]{0:T(1024)} %param.16) | copy-start | bytes 24580
  6.5 39.5 %all-gather.10.cloned.1.call-start = ((), (), s32[]{:S(2)}) async-start(), calls=%async_computation.2 | async-start | bytes 2359296 | tf_op jit(solution)/shard_map/all_gather | solution.py:69
  7.3 123.7 %all-gather.8.cloned.1.call-start = ((), (), s32[]{:S(2)}) async-start(), calls=%async_computation.1 | async-start | bytes 3727360 | tf_op jit(solution)/shard_map/all_gather | solution.py:86
  11.8 165.1 %all-gather.12.cloned.1.call-start = ((), (), s32[]{:S(2)}) async-start(), calls=%async_computation.3 | async-start | bytes 2359296 | tf_op jit(solution)/shard_map/all_gather | solution.py:42
  46.0 85.0 %copy-start.2 = (bf16[1,512,2048]{2,1,0:T(8,128)(2,1)S(1)}, bf16[1,512,2048]{2,1,0:T(8,128)(2,1)}, u32[]{:S(2)}) copy-start(bf16[1,512,2048]{2,1,0:T(8,128)(2,1)} %all-gather.10.cloned.1.call-done) | copy-start | bytes 6291460
  134.3 2.5 copy-start.5
  136.7 87.2 %all-gather.14.cloned.1.call-start = ((), (), s32[]{:S(2)}) async-start(), calls=%async_computation.4 | async-start | bytes 2359296 | tf_op jit(solution)/shard_map/all_gather | solution.py:42
  137.1 44.7 %collective-permute-start = (bf16[4,128,128]{1,2,0:T(8,128)(2,1)S(1)}, bf16[4,128,128]{1,2,0:T(8,128)(2,1)S(1)}, u32[]{:S(2)}, u32[]{:S(2)}) collective-permute-start(bf16[4,128,128]{1,2,0:T(8,128)(2,1)S(1)} %bitcast.236), channel_id=1, source_target_pairs={{0,8},{8,16},{16,24},{24,32},{32,40},{40,48},{48,56},{56,64},{64,7... | collective-permute-start | bytes 393224 | tf_op jit(solution)/shard_map/ppermute | solution.py:122
  182.6 43.0 %copy-start.1 = (f32[32,64,129]{2,1,0:T(8,128)S(1)}, f32[32,64,129]{2,1,0:T(8,128)}, u32[]{:S(2)}) copy-start(f32[32,64,129]{2,1,0:T(8,128)} %all-gather.12.cloned.1.call-done) | copy-start | bytes 3170308
  225.5 2.5 copy-start.3
Sparse Core Ops, SparseCore 0:
  9.5 36.4 all-gather.9
  49.0 81.8 all-gather.7
  136.8 40.0 all-gather.11
  181.1 42.7 all-gather.13
